TPU v7x, 512 devices: a 4x2x32 block of a 4x8x32 slice. The times are simulated.
512 devices in a mesh: grp: 2 (over y), ep: 64 (over z, core), tp: 4 (over x).
Axes of the slice: x: 4, y: 2, z: 32, core: 2. Of those that a mesh axis runs over, the one named last changes fastest.
The devices are a block of a 4x8x32 slice.
Arguments:
- tokens: bfloat16 [24576, 2048], P(('grp', 'ep')), parts along dimension 0, may hold values from -6 to 6
- norm_gain: float32 [2048], replicated, may hold values from 0.1 to 1.9
- w_gate: bfloat16 [64, 2048, 1024], P('ep', None, 'tp'), may hold values from -0.3125 to 0.3125
- w_up: bfloat16 [64, 2048, 1024], P('ep', None, 'tp'), may hold values from -0.3125 to 0.3125
- w_down: bfloat16 [64, 1024, 2048], P('ep', 'tp'), may hold values from -0.09375 to 0.09375
- expert_ids: int32 [24576, 4], P(('grp', 'ep')), parts along dimension 0, may hold values from 0 to 63, all different within a row; in each aligned block of 192 rows (0 to 191, 192 to 383, ...) at most 16 rows name the same one
- gate_weights: float32 [24576, 4], P(('grp', 'ep')), parts along dimension 0, may hold values from 0.1 to 1
Outputs:
- mixed: bfloat16 [24576, 2048], P(('grp', 'ep'), 'tp'), parts along dimension 0
There are 2 independent parts, one for each index of `grp`. A program takes and returns all parts, laid end to end along the dimension named above; an argument that names none is the same for every part. Nothing has to cross between parts.
Inputs may be any that keep to these rules, and one draw needn't show every extreme that they name: `expert_ids`: each row names 4 different experts; among the rows of one index of ep, no expert is named by more than 16 rows, a bound that some block reaches.
All inputs are finite; a program needn't handle non-finite values.
Results may differ from a plain program's by a relative error of at most 0.012.
Values may be sent and summed in bfloat16 or wider, within the bound.
A program may use at most 64 MiB of HBM per device.

v0:
```python
import jax
import jax.numpy as jnp
from jax import lax
from jax.sharding import Mesh
from jax.sharding import PartitionSpec as P

EP = ("ep_0", "ep_1")
GRP_EP = ("grp", "ep_0", "ep_1")
epsilon = 1e-06
clamp_limit = 7.0
swish_alpha = 1.702


def cut_along(value, dim, devices):
    before, after = (value.shape[:dim], value.shape[dim + 1 :])
    return jnp.moveaxis(value.reshape(*before, devices, -1, *after), dim, 0)


def laid_out(blocks, dim):
    blocks = jnp.moveaxis(blocks, 0, dim)
    shape = blocks.shape
    return blocks.reshape(*shape[:dim], shape[dim] * shape[dim + 1], *shape[dim + 2 :])


def turned_blocks(blocks, axes, turns):
    inside = blocks.shape[1:]
    whole = blocks.reshape(*(lax.axis_size(a) for a in axes), *inside)
    for k in turns:
        whole = lax.all_to_all(whole, axes[k], k, k, tiled=True)
    return whole.reshape(-1, *inside)


def exchange_by_chip(value, groups, turns, split_dim, concat_dim):
    devices = lax.axis_size(groups[0]) * lax.axis_size(groups[1])
    blocks = cut_along(value, split_dim, devices)
    return laid_out(turned_blocks(blocks, groups, turns), concat_dim)


def sent_and_summed(value, axis, dim):
    blocks = cut_along(value, dim, lax.axis_size(axis))
    arrived = lax.all_to_all(blocks, axis, split_axis=0, concat_axis=0, tiled=True)
    return arrived.astype(jnp.float32).sum(axis=0)


def rms_norm(tokens, norm_gain):
    widened = tokens.astype(jnp.float32)
    scaled = widened * lax.rsqrt(jnp.mean(widened * widened, axis=-1, keepdims=True) + epsilon)
    return (scaled * norm_gain).astype(jnp.bfloat16)


def body(tokens, norm_gain, w_gate, w_up, w_down, expert_ids, gate_weights):
    tok_rows, model_width = tokens.shape
    top_count = expert_ids.shape[1]
    ep_count = lax.axis_size(EP)
    tp_count = lax.axis_size("tp")
    local_experts = w_gate.shape[0]
    experts_all = local_experts * ep_count
    capacity = min(tok_rows, tok_rows * top_count * 4 // (3 * experts_all))
    normed = rms_norm(tokens, norm_gain)
    flat_ids = expert_ids.reshape(-1)
    onehot = (flat_ids[:, None] == jnp.arange(experts_all, dtype=jnp.int32)[None, :]).astype(
        jnp.int32
    )
    before = jnp.cumsum(onehot, axis=0) - onehot
    slot_index = jnp.sum(before * onehot, axis=1)
    dest_row = flat_ids * capacity + slot_index
    owner_tok = jnp.arange(tok_rows * top_count, dtype=jnp.int32) // top_count
    slot_table = (
        jnp.full((experts_all * capacity,), tok_rows, jnp.int32).at[dest_row].set(owner_tok)
    )
    padded = jnp.concatenate([normed, jnp.zeros((1, model_width), jnp.bfloat16)], axis=0)
    send_buffer = padded[slot_table].reshape(experts_all, capacity, model_width)
    col_share = model_width // tp_count
    col_part = lax.dynamic_slice_in_dim(send_buffer, lax.axis_index("tp") * col_share, col_share, 2)
    received = exchange_by_chip(col_part, ("ep_0", "ep_1"), (1, 0), 0, 0)
    received = lax.all_gather(received, "tp", axis=2, tiled=True)
    expert_rows = received.reshape(ep_count, local_experts, capacity, model_width)
    gate_pre = jnp.einsum("sjcd,jdf->sjcf", expert_rows, w_gate, preferred_element_type=jnp.float32)
    up_pre = jnp.einsum("sjcd,jdf->sjcf", expert_rows, w_up, preferred_element_type=jnp.float32)
    gated = jnp.minimum(gate_pre, clamp_limit)
    linear = jnp.clip(up_pre, -clamp_limit, clamp_limit)
    activated = (gated * jax.nn.sigmoid(swish_alpha * gated) * (linear + 1.0)).astype(jnp.bfloat16)
    partial_value = jnp.einsum(
        "sjcf,jfd->sjcd", activated, w_down, preferred_element_type=jnp.float32
    ).astype(jnp.bfloat16)
    summed = sent_and_summed(partial_value, "tp", 3).astype(jnp.bfloat16)
    returned = exchange_by_chip(summed, ("ep_0", "ep_1"), (1, 0), 0, 0)
    returned = returned.reshape(experts_all * capacity, returned.shape[3])
    picked = returned[dest_row].reshape(tok_rows, top_count, returned.shape[1]).astype(jnp.float32)
    return jnp.sum(picked * gate_weights[:, :, None], axis=1).astype(jnp.bfloat16)


def solution(mesh):
    torus = Mesh(
        mesh.devices.reshape(mesh.shape["grp"], 32, 2, mesh.shape["tp"]),
        ("grp", "ep_0", "ep_1", "tp"),
    )
    return jax.shard_map(
        body,
        mesh=torus,
        in_specs=(
            P(GRP_EP, None),
            P(),
            P(EP, None, "tp"),
            P(EP, None, "tp"),
            P(EP, "tp", None),
            P(GRP_EP, None),
            P(GRP_EP, None),
        ),
        out_specs=P(GRP_EP, "tp"),
        check_vma=False,
    )
```

profile of v0, /device:TPU:33, one launch (start us, length us, event | category | flops | bytes accessed | tf_op | source)
XLA Modules:
  0.0 449.6 jit_solution(9208010235505050856)
XLA Ops:
  6.5 0.0 copy-start
  6.6 0.0 all-gather.2.cloned.1.call-start
  6.6 0.9 copy.23
  7.4 0.1 eq.29
  7.6 0.1 eq.25
  7.7 0.7 broadcast_multiply_fusion
  8.4 1.8 reduce-window.6
  10.2 0.3 slice_reduce_fusion
  10.5 0.1 copy.22
  10.6 0.1 mul.68
  10.7 0.1 fusion.26
  10.9 3.4 scatter_custom_fusion
  14.3 1.4 fusion
  15.7 1.4 fusion.2
  17.1 0.1 concatenate.3
  17.2 6.0 %gather_fusion = bf16[1024,2048]{1,0:T(8,128)(2,1)} fusion(bf16[193,2048]{1,0:T(8,128)(2,1)S(1)} %concatenate.3, s32[1024]{0:T(1024)S(1)} %fusion.30), kind=kCustom, calls=%fused_computation | custom fusion | bytes 8392704 | tf_op jit(solution)/shard_map/gather | solution.py:72
  23.2 1.3 constant_dynamic-slice_fusion
  24.5 0.1 copy.26
  24.6 0.0 copy-start.2
  24.6 45.8 %all_to_all.25 = bf16[32,2,1,16,512]{4,3,0,2,1:T(8,128)(2,1)S(1)} all-to-all(bf16[32,2,1,16,512]{4,3,0,2,1:T(8,128)(2,1)S(1)} %copy.26), channel_id=1, replica_groups=mesh['grp'=2,'ep_0'=32,'ep_1'=2,'tp'=4] {'ep_1'}, dimensions={1} | all-to-all | bytes 2097152 | tf_op jit(solution)/shard_map/all_to_all | solution.py:29
  70.4 0.1 copy.27
  70.5 110.0 %all_to_all.26 = bf16[32,2,1,16,512]{4,3,1,2,0:T(8,128)(2,1)} all-to-all(bf16[32,2,1,16,512]{4,3,1,2,0:T(8,128)(2,1)S(1)} %copy.27), channel_id=1, replica_groups=mesh['grp'=2,'ep_0'=32,'ep_1'=2,'tp'=4] {'ep_0'}, dimensions={0} | all-to-all | bytes 2097152 | tf_op jit(solution)/shard_map/all_to_all | solution.py:29
  180.5 0.0 copy-start.3
  180.5 0.1 all-gather.2.cloned.1.call-update
  180.5 51.5 %all-gather.2.cloned.1.call-done = bf16[64,16,2048]{2,1,0:T(8,128)(2,1)} async-done(((bf16[64,16,512]{2,1,0:T(8,128)(2,1)}), bf16[64,16,2048]{2,1,0:T(8,128)(2,1)}) %all-gather.2.cloned.1.call-update) | async-done | bytes 4194320 | tf_op jit(solution)/shard_map/all_gather | solution.py:76
  232.1 0.0 copy-done.2
  232.1 4.5 %fusion.3 = f32[64,1,16,256]{3,2,0,1:T(8,128)} fusion(bf16[64,16,2048]{2,1,0:T(8,128)(2,1)} %all-gather.2.cloned.1.call-done, bf16[1,2048,256]{2,1,0:T(8,128)(2,1)S(1)} %copy-done.2), kind=kOutput, calls=%fused_computation.12 | convolution fusion | flops 1074003968 | bytes 6291456 | tf_op jit(solution)/shard_map/sjcd,jdf->sjcf/dot_general | solution.py:78
  236.6 0.0 copy-done
  236.6 0.0 copy-done.3
  236.6 8.9 %convolution_convert_fusion = bf16[64,16,2048]{2,1,0:T(8,128)(2,1)} fusion(bf16[64,16,2048]{2,1,0:T(8,128)(2,1)} %all-gather.2.cloned.1.call-done, bf16[1,256,2048]{2,1,0:T(8,128)(2,1)S(1)} %copy-done, bf16[1,2048,256]{2,1,0:T(8,128)(2,1)S(1)} %copy-done.3, f32[64,1,16,256]{3,2,0,1:T(8,128)} %fusion.3), kind=kOutput, calls=%fused_computation.4 | convolution fusion | flops 2151940096 | bytes 11534336 | tf_op jit(solution)/shard_map/sjcf,jfd->sjcd/dot_general | solution.py:83
  245.4 2.8 copy.36
  248.3 51.3 %all_to_all.27 = bf16[4,64,1,16,512]{4,3,1,2,0:T(8,128)(2,1)} all-to-all(bf16[4,64,1,16,512]{4,3,1,2,0:T(8,128)(2,1)S(1)} %bitcast.77), channel_id=1, replica_groups=mesh['grp'=2,'ep_0'=32,'ep_1'=2,'tp'=4] {'tp'}, dimensions={0} | all-to-all | bytes 8388608 | tf_op jit(solution)/shard_map/all_to_all | solution.py:41
  299.6 3.3 reduce_sum.44
  302.9 0.0 copy-start.1
  302.9 0.1 copy.29
  303.0 6.1 %all_to_all.28 = bf16[32,2,1,1,16,512]{5,4,0,3,2,1:T(8,128)(2,1)S(1)} all-to-all(bf16[32,2,1,1,16,512]{5,4,0,3,2,1:T(8,128)(2,1)S(1)} %copy.29), channel_id=1, replica_groups=mesh['grp'=2,'ep_0'=32,'ep_1'=2,'tp'=4] {'ep_1'}, dimensions={1} | all-to-all | bytes 2097152 | tf_op jit(solution)/shard_map/all_to_all | solution.py:29
  309.1 1.1 copy.30
  310.2 23.4 %all-to-all-start.4 = ((bf16[32,2,1,1,16,512]{5,4,1,3,2,0:T(8,128)(2,1)}), bf16[32,2,1,1,16,512]{5,4,1,3,2,0:T(8,128)(2,1)S(1)}, u32[]{:S(2)}, u32[]{:S(2)}) async-start(bf16[32,2,1,1,16,512]{5,4,1,3,2,0:T(8,128)(2,1)} %copy.30), calls=%async_computation.4 | async-start | bytes 2097152 | tf_op jit(solution)/shard_map/all_to_all | solution.py:29
  333.6 0.0 copy-done.1
  333.6 0.1 copy.31
  333.7 104.2 %all-to-all-done.4 = bf16[32,2,1,1,16,512]{5,4,1,3,2,0:T(8,128)(2,1)S(1)} async-done(((bf16[32,2,1,1,16,512]{5,4,1,3,2,0:T(8,128)(2,1)}), bf16[32,2,1,1,16,512]{5,4,1,3,2,0:T(8,128)(2,1)S(1)}, u32[]{:S(2)}, u32[]{:S(2)}) %all-to-all-start.4) | async-done | bytes 1048608 | tf_op jit(solution)/shard_map/all_to_all | solution.py:29
  437.9 2.7 gather_fusion.1
  440.6 0.5 reshape.102
  441.1 1.7 multiply_reduce_fusion
  (7 shorter events, 0.1 us)
Async XLA Ops:
  6.5 230.0 %copy-start = (bf16[1,256,2048]{2,1,0:T(8,128)(2,1)S(1)}, bf16[1,256,2048]{2,1,0:T(8,128)(2,1)}, u32[]{:S(2)}) copy-start(bf16[1,256,2048]{2,1,0:T(8,128)(2,1)} %param.11) | copy-start | bytes 3145732
  6.6 225.5 %all-gather.2.cloned.1.call-start = ((), (), s32[]{:S(2)}) async-start(), calls=%async_computation.5 | async-start | bytes 5242880 | tf_op jit(solution)/shard_map/all_gather | solution.py:76
  24.6 207.5 %copy-start.2 = (bf16[1,2048,256]{2,1,0:T(8,128)(2,1)S(1)}, bf16[1,2048,256]{2,1,0:T(8,128)(2,1)}, u32[]{:S(2)}) copy-start(bf16[1,2048,256]{2,1,0:T(8,128)(2,1)} %param.9) | copy-start | bytes 3145732
  180.5 56.1 %copy-start.3 = (bf16[1,2048,256]{2,1,0:T(8,128)(2,1)S(1)}, bf16[1,2048,256]{2,1,0:T(8,128)(2,1)}, u32[]{:S(2)}) copy-start(bf16[1,2048,256]{2,1,0:T(8,128)(2,1)} %param.10) | copy-start | bytes 3145732
  302.9 30.7 %copy-start.1 = (f32[192,4]{0,1:T(4,128)S(1)}, f32[192,4]{0,1:T(4,128)}, u32[]{:S(2)}) copy-start(f32[192,4]{0,1:T(4,128)} %param.13) | copy-start | bytes 9220
  310.2 127.7 %all-to-all-start.4 = ((bf16[32,2,1,1,16,512]{5,4,1,3,2,0:T(8,128)(2,1)}), bf16[32,2,1,1,16,512]{5,4,1,3,2,0:T(8,128)(2,1)S(1)}, u32[]{:S(2)}, u32[]{:S(2)}) async-start(bf16[32,2,1,1,16,512]{5,4,1,3,2,0:T(8,128)(2,1)} %copy.30), calls=%async_computation.4 | async-start | bytes 2097152 | tf_op jit(solution)/shard_map/all_to_all | solution.py:29
Sparse Core Ops, SparseCore 0:
  180.7 51.3 all-gather.1
where the time goes:
time: 450 us
  blocking collectives  213 us (47%)
  waiting for transfers between devices  156 us (35%)
  starting transfers between devices  23.4 us (5%)
  local copies, waits for them, and re-layouts  19.8 us (4%)
  between operations  13.6 us (3%)
  matrix products  13.4 us (3%)
  other arithmetic  10.5 us (2%)
    all_to_all x3, blocking collectives, turned_blocks(): whole = lax.all_to_all(whole, axes[k], k, k, tiled=True)  162 us
    all_to_all x1, waiting for transfers between devices, turned_blocks(): whole = lax.all_to_all(whole, axes[k], k, k, tiled=True)  104 us
    all_gather x1, waiting for transfers between devices, body(): received = lax.all_gather(received, 'tp', axis=2, tiled=True)  51.5 us
    all_to_all x1, blocking collectives, sent_and_summed(): lax.all_to_all(blocks, axis, split_axis=0, concat_axis=0, tiled=True)  51.3 us
    all_to_all x1, starting transfers between devices, turned_blocks(): whole = lax.all_to_all(whole, axes[k], k, k, tiled=True)  23.4 us
  transfers between devices with their start and end apart: 2, of which 2 were waited for; matrix products, arithmetic and copies ran while one was open for 0% of the time, Pallas kernels for 0%

commit v1 on v0

--- a/solution.py
+++ b/solution.py
@@ -9,6 +9,13 @@
 epsilon = 1e-06
 clamp_limit = 7.0
 swish_alpha = 1.702
+
+
+def make_pairs_all(patch):
+    return jnp.concatenate(
+        lax.all_to_all(jnp.stack(lax.axis_size("tp") * [patch]), "tp", split_axis=0, concat_axis=0),
+        axis=2,
+    )
 
 
 def cut_along(value, dim, devices):
@@ -73,7 +80,7 @@
     col_share = model_width // tp_count
     col_part = lax.dynamic_slice_in_dim(send_buffer, lax.axis_index("tp") * col_share, col_share, 2)
     received = exchange_by_chip(col_part, ("ep_0", "ep_1"), (1, 0), 0, 0)
-    received = lax.all_gather(received, "tp", axis=2, tiled=True)
+    received = make_pairs_all(received)
     expert_rows = received.reshape(ep_count, local_experts, capacity, model_width)
     gate_pre = jnp.einsum("sjcd,jdf->sjcf", expert_rows, w_gate, preferred_element_type=jnp.float32)
     up_pre = jnp.einsum("sjcd,jdf->sjcf", expert_rows, w_up, preferred_element_type=jnp.float32)

time: 450 us -> 422 us (0.938)
  blocking collectives: 213 us -> 265 us
  waiting for transfers between devices: 156 us -> 105 us
  starting transfers between devices: 23.4 us -> 7.93 us
  between operations: 13.6 us -> 0.23 us
    all_to_all x0 -> x1, blocking collectives: none -> 52 us  [make_pairs_all(): lax.all_to_all(jnp.stack(lax.axis_size('tp') * [patch]), 'tp', split_axis...]
    all_gather x1 -> x0, waiting for transfers between devices: 51.5 us -> none  [body(): received = lax.all_gather(received, 'tp', axis=2, tiled=True)]
    all_to_all x1, starting transfers between devices: 23.4 us -> 7.93 us  [turned_blocks(): whole = lax.all_to_all(whole, axes[k], k, k, tiled=True)]
  transfers between devices with their start and end apart: 2 -> 1, of which waited for: 2 -> 1; matrix products, arithmetic and copies ran while one was open for 0% -> 0% of each run, Pallas kernels for 0% -> 0%
where the time goes in v1:
time: 422 us; the launch traced here: 421 us
  blocking collectives  265 us (63%)
  waiting for transfers between devices  105 us (25%)
  local copies, waits for them, and re-layouts  22.9 us (5%)
  other arithmetic  10.5 us (2%)
  matrix products  9.82 us (2%)
  starting transfers between devices  7.93 us (2%)
    all_to_all x3, blocking collectives, turned_blocks(): whole = lax.all_to_all(whole, axes[k], k, k, tiled=True)  163 us
    all_to_all x1, waiting for transfers between devices, turned_blocks(): whole = lax.all_to_all(whole, axes[k], k, k, tiled=True)  105 us
    all_to_all x1, blocking collectives, make_pairs_all(): lax.all_to_all(jnp.stack(lax.axis_size('tp') * [patch]), 'tp', split_axis...  52 us
    all_to_all x1, blocking collectives, sent_and_summed(): lax.all_to_all(blocks, axis, split_axis=0, concat_axis=0, tiled=True)  50.5 us
    dot_general x1, matrix products, body(): jnp.einsum('sjcf,jfd->sjcd', activated, w_down, preferred_element_type=jn...  8.57 us
  transfers between devices with their start and end apart: 1, of which 1 were waited for; matrix products, arithmetic and copies ran while one was open for 0% of the time, Pallas kernels for 0%

profile of v1, /device:TPU:33, one launch (start us, length us, event | category | flops | bytes accessed | tf_op | source)
XLA Modules:
  0.0 420.9 jit_solution(46805678572778544)
XLA Ops:
  0.0 0.0 copy-start
  0.0 0.9 copy.24
  0.9 0.1 eq.29
  1.0 0.1 eq.25
  1.1 0.7 broadcast_multiply_fusion
  1.8 1.8 reduce-window.6
  3.6 0.3 slice_reduce_fusion
  3.9 0.1 copy.23
  4.1 0.1 mul.68
  4.2 0.1 fusion.26
  4.3 3.4 scatter_custom_fusion
  7.7 1.4 fusion
  9.1 1.4 fusion.2
  10.5 0.1 concatenate.3
  10.6 6.0 %gather_fusion = bf16[1024,2048]{1,0:T(8,128)(2,1)} fusion(bf16[193,2048]{1,0:T(8,128)(2,1)S(1)} %concatenate.3, s32[1024]{0:T(1024)S(1)} %fusion.30), kind=kCustom, calls=%fused_computation | custom fusion | bytes 8392704 | tf_op jit(solution)/shard_map/gather | solution.py:79
  16.6 1.3 constant_dynamic-slice_fusion
  17.9 0.1 copy.27
  18.0 45.6 %all_to_all.30 = bf16[32,2,1,16,512]{4,3,0,2,1:T(8,128)(2,1)S(1)} all-to-all(bf16[32,2,1,16,512]{4,3,0,2,1:T(8,128)(2,1)S(1)} %copy.27), channel_id=1, replica_groups=mesh['grp'=2,'ep_0'=32,'ep_1'=2,'tp'=4] {'ep_1'}, dimensions={1} | all-to-all | bytes 2097152 | tf_op jit(solution)/shard_map/all_to_all | solution.py:36
  63.7 0.1 copy.28
  63.8 109.9 %all_to_all.31 = bf16[32,2,1,16,512]{4,3,1,2,0:T(8,128)(2,1)S(1)} all-to-all(bf16[32,2,1,16,512]{4,3,1,2,0:T(8,128)(2,1)S(1)} %copy.28), channel_id=1, replica_groups=mesh['grp'=2,'ep_0'=32,'ep_1'=2,'tp'=4] {'ep_0'}, dimensions={0} | all-to-all | bytes 2097152 | tf_op jit(solution)/shard_map/all_to_all | solution.py:36
  173.7 0.6 stack.3
  174.2 52.0 %all_to_all.32 = bf16[4,64,16,512]{3,2,1,0:T(8,128)(2,1)S(1)} all-to-all(bf16[4,64,16,512]{3,2,1,0:T(8,128)(2,1)S(1)} %stack.3), channel_id=1, replica_groups=mesh['grp'=2,'ep_0'=32,'ep_1'=2,'tp'=4] {'tp'}, dimensions={0} | all-to-all | bytes 8388608 | tf_op jit(solution)/shard_map/all_to_all | solution.py:16
  226.2 0.0 copy-start.3
  226.2 0.6 copy.36
  226.9 0.0 copy-start.1
  226.9 0.0 copy-start.4
  226.9 1.9 copy-done.1
  228.8 0.0 copy-done.3
  228.8 1.3 fusion.3
  230.1 0.0 copy-done
  230.1 0.0 copy-done.4
  230.1 8.6 %convolution_convert_fusion = bf16[64,16,2048]{2,1,0:T(8,128)(2,1)} fusion(bf16[64,16,2048]{2,1,0:T(8,128)(2,1)} %bitcast.86, bf16[1,256,2048]{2,1,0:T(8,128)(2,1)S(1)} %copy-done, bf16[1,2048,256]{2,1,0:T(8,128)(2,1)S(1)} %copy-done.4, f32[64,1,16,256]{3,2,0,1:T(8,128)S(1)} %fusion.3), kind=kOutput, calls=%fused_computation.4 | convolution fusion | flops 2151940096 | bytes 11534336 | tf_op jit(solution)/shard_map/sjcf,jfd->sjcd/dot_general | solution.py:90
  238.7 2.8 copy.39
  241.5 50.5 %all_to_all.33 = bf16[4,64,1,16,512]{4,3,1,2,0:T(8,128)(2,1)} all-to-all(bf16[4,64,1,16,512]{4,3,1,2,0:T(8,128)(2,1)S(1)} %bitcast.81), channel_id=1, replica_groups=mesh['grp'=2,'ep_0'=32,'ep_1'=2,'tp'=4] {'tp'}, dimensions={0} | all-to-all | bytes 8388608 | tf_op jit(solution)/shard_map/all_to_all | solution.py:48
  292.0 3.3 reduce_sum.44
  295.3 0.0 copy-start.2
  295.3 0.1 copy.31
  295.4 6.9 %all_to_all.34 = bf16[32,2,1,1,16,512]{5,4,0,3,2,1:T(8,128)(2,1)S(1)} all-to-all(bf16[32,2,1,1,16,512]{5,4,0,3,2,1:T(8,128)(2,1)S(1)} %copy.31), channel_id=1, replica_groups=mesh['grp'=2,'ep_0'=32,'ep_1'=2,'tp'=4] {'ep_1'}, dimensions={1} | all-to-all | bytes 2097152 | tf_op jit(solution)/shard_map/all_to_all | solution.py:36
  302.4 1.1 copy.32
  303.4 7.9 %all-to-all-start.5 = ((bf16[32,2,1,1,16,512]{5,4,1,3,2,0:T(8,128)(2,1)}), bf16[32,2,1,1,16,512]{5,4,1,3,2,0:T(8,128)(2,1)S(1)}, u32[]{:S(2)}, u32[]{:S(2)}) async-start(bf16[32,2,1,1,16,512]{5,4,1,3,2,0:T(8,128)(2,1)} %copy.32), calls=%async_computation.5 | async-start | bytes 2097152 | tf_op jit(solution)/shard_map/all_to_all | solution.py:36
  311.4 0.0 copy-done.2
  311.4 0.1 copy.33
  311.5 104.5 %all-to-all-done.5 = bf16[32,2,1,1,16,512]{5,4,1,3,2,0:T(8,128)(2,1)S(1)} async-done(((bf16[32,2,1,1,16,512]{5,4,1,3,2,0:T(8,128)(2,1)}), bf16[32,2,1,1,16,512]{5,4,1,3,2,0:T(8,128)(2,1)S(1)}, u32[]{:S(2)}, u32[]{:S(2)}) %all-to-all-start.5) | async-done | bytes 1048608 | tf_op jit(solution)/shard_map/all_to_all | solution.py:36
  416.0 2.7 gather_fusion.1
  418.7 0.5 reshape.110
  419.2 1.7 multiply_reduce_fusion
  (7 shorter events, 0.1 us)
Async XLA Ops:
  0.0 230.1 %copy-start = (bf16[1,256,2048]{2,1,0:T(8,128)(2,1)S(1)}, bf16[1,256,2048]{2,1,0:T(8,128)(2,1)}, u32[]{:S(2)}) copy-start(bf16[1,256,2048]{2,1,0:T(8,128)(2,1)} %param.11) | copy-start | bytes 3145732
  226.2 2.6 copy-start.3
  226.9 1.9 copy-start.1
  226.9 3.2 copy-start.4
  295.3 16.1 %copy-start.2 = (f32[192,4]{0,1:T(4,128)S(1)}, f32[192,4]{0,1:T(4,128)}, u32[]{:S(2)}) copy-start(f32[192,4]{0,1:T(4,128)} %param.13) | copy-start | bytes 9220
  303.4 112.6 %all-to-all-start.5 = ((bf16[32,2,1,1,16,512]{5,4,1,3,2,0:T(8,128)(2,1)}), bf16[32,2,1,1,16,512]{5,4,1,3,2,0:T(8,128)(2,1)S(1)}, u32[]{:S(2)}, u32[]{:S(2)}) async-start(bf16[32,2,1,1,16,512]{5,4,1,3,2,0:T(8,128)(2,1)} %copy.32), calls=%async_computation.5 | async-start | bytes 2097152 | tf_op jit(solution)/shard_map/all_to_all | solution.py:36
